TPU v7x, 32 devices: a whole 2x2x4 slice. The times are simulated.
32 devices in a mesh: ep: 8 (over z, x), tp: 4 (over y, core).
Axes of the slice: x: 2, y: 2, z: 4, core: 2. Of those that a mesh axis runs over, the one named last changes fastest.
Arguments:
- conv_input: bfloat16 [8192, 2048], P('ep', 'tp'), may hold values from -6 to 6
- conv_kernel: bfloat16 [31, 2048], P(None, 'tp'), may hold values from -2 to 2
- norm_gain: float32 [2048], P('tp'), may hold values from 0.1 to 1.9
- norm_shift: float32 [2048], P('tp'), may hold values from -3 to 3
- conv_proj: bfloat16 [2048, 2048], P('tp'), may hold values from -0.125 to 0.125
- moe_input: bfloat16 [2048, 2048], P(('ep', 'tp')), may hold values from -6 to 6
- moe_gain: float32 [2048], replicated, may hold values from 0.1 to 1.9
- routes: int32 [2048, 2], P('ep'), may hold values from 0 to 7, all different within a row; in each aligned block of 256 rows (0 to 255, 256 to 511, ...) at most 128 rows name the same one
- route_weights: float32 [2048, 2], P('ep'), may hold values from 0.2 to 1
- gate_proj: bfloat16 [8, 2048, 2048], P('ep', None, 'tp'), may hold values from -0.125 to 0.125
- up_proj: bfloat16 [8, 2048, 2048], P('ep', None, 'tp'), may hold values from -0.125 to 0.125
- down_proj: bfloat16 [8, 2048, 2048], P('ep', 'tp'), may hold values from -0.125 to 0.125
Outputs:
- conv_out: bfloat16 [8192, 2048], P(('ep', 'tp'))
- moe_out: bfloat16 [2048, 2048], P(('ep', 'tp'))
Inputs may be any that keep to these rules, and one draw needn't show every extreme that they name: `routes`: each row names 2 different experts. In each aligned block of 256 rows no expert is named by more than 128 rows, and in some blocks an expert is named by exactly 128 rows.
All inputs are finite; a program needn't handle non-finite values.
Results may differ from a plain program's by a relative error of at most 0.012.
Values may be sent and summed in bfloat16 or wider, within the bound.
A program may use at most 128 MiB of HBM per device.

v0:
```python
import jax
import jax.numpy as jnp
from jax import lax
from jax.sharding import PartitionSpec as P


def shifted(value, axis, steps):
    count = lax.axis_size(axis)
    leading, last = (max(0, -steps), min(count, count - steps))
    return lax.ppermute(value, axis, [(source, source + steps) for source in range(leading, last)])


def local(
    conv_input,
    conv_kernel,
    norm_gain,
    norm_shift,
    conv_proj,
    moe_input,
    moe_gain,
    routes,
    route_weights,
    gate_proj,
    up_proj,
    down_proj,
):
    tp_count = lax.axis_size("tp")
    ep_count = lax.axis_size("ep")
    local_rows, local_width = conv_input.shape
    reach = conv_kernel.shape[0] - 1
    history = shifted(conv_input[local_rows - reach :], "ep", 1)
    padded = jnp.concatenate([history, conv_input], axis=0)
    taps = conv_kernel.astype(jnp.float32)
    mixed = jnp.zeros((local_rows, local_width), jnp.float32)
    for offset in range(reach + 1):
        mixed = mixed + padded[offset : offset + local_rows].astype(jnp.float32) * taps[offset]
    full_width = local_width * tp_count
    sums, squares = lax.psum((jnp.sum(mixed, axis=1), jnp.sum(mixed * mixed, axis=1)), "tp")
    center = sums / full_width
    spread = jnp.maximum(squares / full_width - center * center, 0.0)
    scaled = (mixed - center[:, None]) * lax.rsqrt(spread[:, None] + 1e-05) * norm_gain + norm_shift
    activated = jax.nn.silu(scaled).astype(jnp.bfloat16)
    conv_out = lax.psum_scatter(
        jnp.dot(activated, conv_proj, preferred_element_type=jnp.float32).astype(jnp.bfloat16),
        "tp",
        scatter_dimension=0,
        tiled=True,
    )
    moe_float = moe_input.astype(jnp.float32)
    normed = (
        moe_float
        * lax.rsqrt(jnp.mean(moe_float * moe_float, axis=1, keepdims=True) + 1e-06)
        * moe_gain
    ).astype(jnp.bfloat16)
    group = lax.all_gather(normed, "tp", axis=0, tiled=True)
    group_rows, top_count = routes.shape
    model_width = group.shape[1]
    capacity = 2 * top_count * group_rows // ep_count
    expert_ids = routes.reshape(-1)
    onehot = (expert_ids[:, None] == jnp.arange(ep_count, dtype=jnp.int32)[None, :]).astype(
        jnp.int32
    )
    ranks = jnp.sum((jnp.cumsum(onehot, axis=0) - onehot) * onehot, axis=1)
    targets = ranks * ep_count + expert_ids
    owners = jnp.arange(group_rows * top_count, dtype=jnp.int32) // top_count
    table = jnp.full((capacity * ep_count,), group_rows, jnp.int32).at[targets].set(owners)
    extended = jnp.concatenate([group, jnp.zeros((1, model_width), jnp.bfloat16)], axis=0)
    outgoing = extended[table].reshape(capacity, ep_count, model_width)
    share = capacity // tp_count
    own_slots = lax.dynamic_slice_in_dim(outgoing, lax.axis_index("tp") * share, share, 0)
    landed = lax.all_to_all(own_slots, "ep", split_axis=1, concat_axis=1, tiled=True)
    arrived = lax.all_gather(landed, "tp", axis=0, tiled=True)
    incoming = arrived.reshape(capacity * ep_count, model_width)
    gated = jax.nn.silu(jnp.dot(incoming, gate_proj[0], preferred_element_type=jnp.float32))
    hidden = (gated * jnp.dot(incoming, up_proj[0], preferred_element_type=jnp.float32)).astype(
        jnp.bfloat16
    )
    weights_flat = route_weights.reshape(-1)
    pieces = jnp.dot(hidden, down_proj[0], preferred_element_type=jnp.float32).astype(jnp.bfloat16)
    returned = lax.all_to_all(
        pieces.reshape(capacity, ep_count, model_width),
        "ep",
        split_axis=1,
        concat_axis=1,
        tiled=True,
    )
    picked = returned.reshape(-1, model_width)[targets].astype(jnp.float32)
    combined = jnp.sum(
        (picked * weights_flat[:, None]).reshape(group_rows, top_count, model_width), axis=1
    )
    moe_out = lax.psum_scatter(combined.astype(jnp.bfloat16), "tp", scatter_dimension=0, tiled=True)
    return (conv_out, moe_out)


def solution(mesh):
    placed = (
        P("ep", "tp"),
        P(None, "tp"),
        P("tp"),
        P("tp"),
        P("tp", None),
        P(("ep", "tp"), None),
        P(),
        P("ep", None),
        P("ep", None),
        P("ep", None, "tp"),
        P("ep", None, "tp"),
        P("ep", "tp", None),
    )
    return jax.shard_map(
        local,
        mesh=mesh,
        in_specs=placed,
        out_specs=(P(("ep", "tp"), None), P(("ep", "tp"), None)),
        check_vma=False,
    )
```

profile of v0, /device:TPU:0, one launch (start us, length us, event | category | flops | bytes accessed | tf_op | source)
XLA Modules:
  0.0 288.2 jit_solution(171710955497054303)
XLA Ops:
  8.5 1.8 fusion.52
  13.1 2.4 scatter_custom_fusion
  15.6 14.3 %all-gather.3.cloned.1.call-done = bf16[256,2048]{1,0:T(8,128)(2,1)} async-done(((bf16[64,2048]{1,0:T(8,128)(2,1)}), bf16[256,2048]{1,0:T(8,128)(2,1)}) %all-gather.3.cloned.1.call-update) | async-done | bytes 1048592 | tf_op jit(solution)/shard_map/all_gather | solution.py:55
  29.9 1.3 concatenate.7
  31.2 6.0 %gather_fusion = bf16[1024,2048]{1,0:T(8,128)(2,1)} fusion(bf16[257,2048]{1,0:T(8,128)(2,1)S(1)} %concatenate.7, s32[1024]{0:T(1024)S(1)} %fusion.56), kind=kCustom, calls=%fused_computation | custom fusion | bytes 8392704 | tf_op jit(solution)/shard_map/gather | solution.py:68
  37.2 1.3 constant_dynamic-slice_fusion
  39.1 31.4 %all_to_all.10 = bf16[32,8,2048]{2,0,1:T(8,128)(2,1)S(1)} all-to-all(bf16[32,8,2048]{2,0,1:T(8,128)(2,1)S(1)} %copy.27), channel_id=1, replica_groups=mesh['ep'=8,'tp'=4] {'ep'}, dimensions={1} | all-to-all | bytes 2097152 | tf_op jit(solution)/shard_map/all_to_all | solution.py:71
  70.5 1.6 copy.23
  72.2 3.4 %collective-permute-start = (bf16[30,512]{1,0:T(8,128)(2,1)S(1)}, bf16[30,512]{1,0:T(8,128)(2,1)S(1)}, u32[]{:S(2)}, u32[]{:S(2)}) collective-permute-start(bf16[30,512]{1,0:T(8,128)(2,1)S(1)} %slice.192), channel_id=1, source_target_pairs={{0,4},{4,8},{8,12},{12,16},{16,20},{20,24},{24,28},{1,5},{5,9},{9,... | collective-permute-start | bytes 92168 | tf_op jit(solution)/shard_map/ppermute | solution.py:10
  75.6 1.5 collective-permute-done
  77.1 11.2 %fusion.64 = (f32[1024]{0:T(1024)S(1)}, f32[1024]{0:T(1024)S(1)}, f32[1024,512]{1,0:T(8,128)}) fusion(f32[512]{0:T(512)S(1)} %bitcast.105, bf16[1024,512]{1,0:T(8,128)(2,1)S(1)} %copy-done.1, f32[512]{0:T(512)S(1)} %bitcast.104, bf16[30,512]{1,0:T(8,128)(2,1)S(1)} %collective-permute-done, f32[512]{0:T(512)S(1)} %bitcast.103, f32[512]{0:T(512)S(1)} %bitcast.102, ...), kind=kLoop, calls=%fused_computation.119 | loop fusion | flops 96991232 | bytes 3248128 | tf_op jit(solution)/shard_map/reduce_sum | solution.py:38
  88.3 7.0 %all-reduce.1 = (f32[1024]{0:T(1024)S(1)}, f32[1024]{0:T(1024)S(1)}) all-reduce(f32[1024]{0:T(1024)S(1)} %get-tuple-element.3, f32[1024]{0:T(1024)S(1)} %get-tuple-element.2), channel_id=1, replica_groups=mesh['ep'=8,'tp'=4] {'tp'}, use_global_device_ids=true, to_apply=%region_3.0 | all-reduce | flops 2048 | bytes 16384 | tf_op jit(solution)/shard_map/psum | solution.py:38
  95.3 6.3 %convolution_convert_fusion = bf16[1024,2048]{1,0:T(8,128)(2,1)} fusion(bf16[512,2048]{1,0:T(8,128)(2,1)S(1)} %copy-done, f32[1024,512]{1,0:T(8,128)} %get-tuple-element.6, f32[512]{0:T(512)S(1)} %copy-done.4, f32[512]{0:T(512)S(1)} %copy-done.5, f32[1024]{0:T(1024)S(1)} %get-tuple-element.39, f32[1024]{0:T(1024)S(1)} %get-tuple-element.38), kind=kOutput, calls=%fused_computation.39 | convolution fusion | flops 2154299392 | bytes 8400896 | tf_op jit(solution)/shard_map/dot_general | solution.py:44
  101.6 3.5 %all-gather.5.cloned.1.call-done = bf16[128,8,2048]{2,1,0:T(8,128)(2,1)} async-done(((bf16[32,8,2048]{2,1,0:T(8,128)(2,1)}), bf16[128,8,2048]{2,1,0:T(8,128)(2,1)}) %all-gather.5.cloned.1.call-update) | async-done | bytes 4194320 | tf_op jit(solution)/shard_map/all_gather | solution.py:72
  105.1 6.6 %fusion.2 = f32[1024,512]{1,0:T(8,128)} fusion(bf16[128,8,2048]{2,1,0:T(8,128)(2,1)} %all-gather.5.cloned.1.call-done, bf16[1,2048,512]{2,1,0:T(8,128)(2,1)} %param.21), kind=kOutput, calls=%fused_computation.34 | convolution fusion | flops 2147483648 | bytes 8388608 | tf_op jit(solution)/shard_map/dot_general | solution.py:74
  111.7 11.5 %convert_bitcast_fusion = bf16[128,8,2048]{2,1,0:T(8,128)(2,1)} fusion(bf16[1,512,2048]{2,1,0:T(8,128)(2,1)} %param.23, f32[1024,512]{1,0:T(8,128)} %fusion.2, bf16[1,2048,512]{2,1,0:T(8,128)(2,1)} %param.22, bf16[128,8,2048]{2,1,0:T(8,128)(2,1)} %all-gather.5.cloned.1.call-done), kind=kOutput, calls=%fused_computation.38 | convolution fusion | flops 4300210176 | bytes 14680064 | tf_op jit(solution)/shard_map/dot_general | solution.py:79
  123.2 6.4 %copy.24 = bf16[128,8,2048]{2,0,1:T(8,128)(2,1)} copy(bf16[128,8,2048]{2,1,0:T(8,128)(2,1)} %convert_bitcast_fusion) | data formatting | bytes 8388608 | tf_op jit(solution)/shard_map/reshape | solution.py:81
  129.6 5.4 %all-to-all-start.1 = ((bf16[128,8,2048]{2,0,1:T(8,128)(2,1)}), bf16[128,8,2048]{2,0,1:T(8,128)(2,1)}, u32[]{:S(2)}, u32[]{:S(2)}) async-start(bf16[128,8,2048]{2,0,1:T(8,128)(2,1)} %copy.24), calls=%async_computation.2 | async-start | bytes 8388608 | tf_op jit(solution)/shard_map/all_to_all | solution.py:80
  135.5 93.3 %all-to-all-done.1 = bf16[128,8,2048]{2,0,1:T(8,128)(2,1)} async-done(((bf16[128,8,2048]{2,0,1:T(8,128)(2,1)}), bf16[128,8,2048]{2,0,1:T(8,128)(2,1)}, u32[]{:S(2)}, u32[]{:S(2)}) %all-to-all-start.1) | async-done | bytes 4194336 | tf_op jit(solution)/shard_map/all_to_all | solution.py:80
  228.8 6.5 %copy.29 = bf16[128,8,2048]{2,1,0:T(8,128)(2,1)} copy(bf16[128,8,2048]{2,0,1:T(8,128)(2,1)} %all-to-all-done.1) | data formatting | bytes 8388608 | tf_op jit(solution)/shard_map/all_to_all | solution.py:80
  235.2 8.0 %gather_fusion.1 = bf16[512,2048]{1,0:T(8,128)(2,1)} fusion(bf16[1024,2048]{1,0:T(8,128)(2,1)} %bitcast.70, s32[1024]{0:T(1024)S(1)} %pad_clamp_fusion), kind=kCustom, calls=%fused_computation.1 | custom fusion | bytes 4196352 | tf_op jit(solution)/shard_map/gather | solution.py:87
  243.2 5.4 %reshape.95 = f32[256,2,2048]{2,1,0:T(2,128)} reshape(bf16[512,2048]{1,0:T(8,128)(2,1)} %gather_fusion.1) | data formatting | bytes 6291456 | tf_op jit(solution)/shard_map/convert_element_type | solution.py:87
  248.6 10.0 %multiply_reduce_fusion = bf16[256,2048]{1,0:T(8,128)(2,1)} fusion(f32[256,2,2048]{2,1,0:T(2,128)} %reshape.95, f32[256,2]{1,0:T(8,128)S(1)} %copy.26), kind=kLoop, calls=%fused_computation.37 | loop fusion | flops 1572864 | bytes 5244928 | tf_op jit(solution)/shard_map/reduce_sum | solution.py:88
  258.6 23.0 %reduce-scatter.5.cloned.1.call-done = bf16[64,2048]{1,0:T(8,128)(2,1)} async-done(((bf16[256,2048]{1,0:T(8,128)(2,1)}), bf16[64,2048]{1,0:T(8,128)(2,1)}) %reduce-scatter.5.cloned.1.call-update) | async-done | bytes 262160 | tf_op jit(solution)/shard_map/reduce_scatter | solution.py:91
  (44 shorter events, 5.3 us)
Async XLA Ops:
  7.2 88.1 %copy-start = (bf16[512,2048]{1,0:T(8,128)(2,1)S(1)}, bf16[512,2048]{1,0:T(8,128)(2,1)}, u32[]{:S(2)}) copy-start(bf16[512,2048]{1,0:T(8,128)(2,1)} %param.16) | copy-start | bytes 6291460
  7.2 22.7 %all-gather.3.cloned.1.call-start = ((), (), s32[]{:S(2)}) async-start(), calls=%async_computation.5 | async-start | bytes 1310720 | tf_op jit(solution)/shard_map/all_gather | solution.py:55
  10.3 94.8 %all-gather.5.cloned.1.call-start = ((), (), s32[]{:S(2)}) async-start(), calls=%async_computation.6 | async-start | bytes 5242880 | tf_op jit(solution)/shard_map/all_gather | solution.py:72
  70.5 1.6 copy-start.1
  70.5 5.0 %copy-start.2 = (bf16[31,512]{1,0:T(8,128)(2,1)S(1)}, bf16[31,512]{1,0:T(8,128)(2,1)}, u32[]{:S(2)}) copy-start(bf16[31,512]{1,0:T(8,128)(2,1)} %param.13) | copy-start | bytes 95236
  72.1 23.2 %copy-start.4 = (f32[512]{0:T(512)S(1)}, f32[512]{0:T(512)}, u32[]{:S(2)}) copy-start(f32[512]{0:T(512)} %param.15) | copy-start | bytes 6148
  72.1 23.2 %copy-start.5 = (f32[512]{0:T(512)S(1)}, f32[512]{0:T(512)}, u32[]{:S(2)}) copy-start(f32[512]{0:T(512)} %param.14) | copy-start | bytes 6148
  72.1 186.5 %reduce-scatter.3.cloned.1.call-start = ((), (), s32[]{:S(2)}) async-start(), calls=%async_computation.4 | async-start | bytes 5242880 | tf_op jit(solution)/shard_map/reduce_scatter | solution.py:43
  72.2 5.0 %collective-permute-start = (bf16[30,512]{1,0:T(8,128)(2,1)S(1)}, bf16[30,512]{1,0:T(8,128)(2,1)S(1)}, u32[]{:S(2)}, u32[]{:S(2)}) collective-permute-start(bf16[30,512]{1,0:T(8,128)(2,1)S(1)} %slice.192), channel_id=1, source_target_pairs={{0,4},{4,8},{8,12},{12,16},{16,20},{20,24},{24,28},{1,5},{5,9},{9,... | collective-permute-start | bytes 92168 | tf_op jit(solution)/shard_map/ppermute | solution.py:10
  129.6 5.7 %copy-start.3 = (f32[256,2]{0,1:T(2,128)S(1)}, f32[256,2]{0,1:T(2,128)}, u32[]{:S(2)}) copy-start(f32[256,2]{0,1:T(2,128)} %param.20) | copy-start | bytes 6148
  129.6 99.1 %all-to-all-start.1 = ((bf16[128,8,2048]{2,0,1:T(8,128)(2,1)}), bf16[128,8,2048]{2,0,1:T(8,128)(2,1)}, u32[]{:S(2)}, u32[]{:S(2)}) async-start(bf16[128,8,2048]{2,0,1:T(8,128)(2,1)} %copy.24), calls=%async_computation.2 | async-start | bytes 8388608 | tf_op jit(solution)/shard_map/all_to_all | solution.py:80
  135.1 146.6 %reduce-scatter.5.cloned.1.call-start = ((), (), s32[]{:S(2)}) async-start(), calls=%async_computation.7 | async-start | bytes 1310720 | tf_op jit(solution)/shard_map/reduce_scatter | solution.py:91
Sparse Core Ops, SparseCore 0:
  10.4 19.4 all-gather.2
  72.2 32.8 all-gather.4
  108.2 44.5 reduce-scatter.2
  258.7 22.9 reduce-scatter.4
where the time goes:
time: 289 us; the launch traced here: 288 us
  waiting for transfers between devices  136 us (47%)
  local copies, waits for them, and re-layouts  41.2 us (14%)
  blocking collectives  38.4 us (13%)
  other arithmetic  25.5 us (9%)
  matrix products  24.4 us (8%)
  between operations  14 us (5%)
  starting transfers between devices  9.18 us (3%)
    all_to_all x1, waiting for transfers between devices, local(): lax.all_to_all(pieces.reshape(capacity, ep_count, model_width), 'ep', spl...  93.3 us
    all_to_all x1, blocking collectives, local(): lax.all_to_all(own_slots, 'ep', split_axis=1, concat_axis=1, tiled=True)  31.4 us
    reduce_scatter x1, waiting for transfers between devices, local(): lax.psum_scatter(combined.astype(jnp.bfloat16), 'tp', scatter_dimension=0...  23 us
    all_gather x1, waiting for transfers between devices, local(): group = lax.all_gather(normed, 'tp', axis=0, tiled=True)  14.3 us
    dot_general x1, matrix products, local(): jnp.dot(hidden, down_proj[0], preferred_element_type=jnp.float32)  11.5 us
    reduce_sum x1, other arithmetic, local(): jnp.sum(mixed, axis=1)  11.2 us
    reduce_sum x1, other arithmetic, local(): jnp.sum((picked * weights_flat[:, None]).reshape(group_rows, top_count, m...  9.96 us
    gather x1, local copies, waits for them, and re-layouts, local(): picked = returned.reshape(-1, model_width)[targets].astype(jnp.float32)  7.95 us
  transfers between devices with their start and end apart: 6, of which 5 were waited for; matrix products, arithmetic and copies ran while one was open for 27% of the time, Pallas kernels for 0%

commit v1 on v0

--- a/solution.py
+++ b/solution.py
@@ -77,13 +77,11 @@
     )
     weights_flat = route_weights.reshape(-1)
     pieces = jnp.dot(hidden, down_proj[0], preferred_element_type=jnp.float32).astype(jnp.bfloat16)
-    returned = lax.all_to_all(
-        pieces.reshape(capacity, ep_count, model_width),
-        "ep",
-        split_axis=1,
-        concat_axis=1,
-        tiled=True,
-    )
+    own = pieces.reshape(capacity, ep_count, model_width)
+    size = lax.axis_size("ep")
+    blocks = jnp.stack(jnp.split(own, size, axis=1), axis=0)
+    blocks = lax.all_to_all(blocks, "ep", split_axis=0, concat_axis=0)
+    returned = jnp.concatenate(blocks, axis=1)
     picked = returned.reshape(-1, model_width)[targets].astype(jnp.float32)
     combined = jnp.sum(
         (picked * weights_flat[:, None]).reshape(group_rows, top_count, model_width), axis=1

time: 289 us -> 314 us (1.087)
  local copies, waits for them, and re-layouts: 41.2 us -> 66.7 us
    split x0 -> x1, local copies, waits for them, and re-layouts: none -> 22.6 us  [local(): blocks = jnp.stack(jnp.split(own, size, axis=1), axis=0)]
    unnamed x15 -> x26, local copies, waits for them, and re-layouts: 1.55 us -> 9.39 us
    all_to_all x1 -> x0, local copies, waits for them, and re-layouts: 6.46 us -> none  [local(): lax.all_to_all(pieces.reshape(capacity, ep_count, model_width), 'ep', spl...]
  transfers between devices with their start and end apart: 6 -> 6, of which waited for: 5 -> 5; matrix products, arithmetic and copies ran while one was open for 27% -> 33% of each run, Pallas kernels for 0% -> 0%
where the time goes in v1:
time: 314 us; the launch traced here: 313 us
  waiting for transfers between devices  136 us (43%)
  local copies, waits for them, and re-layouts  66.7 us (21%)
  blocking collectives  38.4 us (12%)
  other arithmetic  25.5 us (8%)
  matrix products  23.5 us (7%)
  between operations  14 us (4%)
  starting transfers between devices  9.18 us (3%)
    all_to_all x1, waiting for transfers between devices, local(): blocks = lax.all_to_all(blocks, 'ep', split_axis=0, concat_axis=0)  93.5 us
    all_to_all x1, blocking collectives, local(): lax.all_to_all(own_slots, 'ep', split_axis=1, concat_axis=1, tiled=True)  31.4 us
    reduce_scatter x1, waiting for transfers between devices, local(): lax.psum_scatter(combined.astype(jnp.bfloat16), 'tp', scatter_dimension=0...  23 us
    split x1, local copies, waits for them, and re-layouts, local(): blocks = jnp.stack(jnp.split(own, size, axis=1), axis=0)  22.6 us
    all_gather x1, waiting for transfers between devices, local(): group = lax.all_gather(normed, 'tp', axis=0, tiled=True)  14.3 us
    dot_general x1, matrix products, local(): jnp.dot(hidden, down_proj[0], preferred_element_type=jnp.float32)  11.3 us
    reduce_sum x1, other arithmetic, local(): jnp.sum(mixed, axis=1)  11.2 us
    reduce_sum x1, other arithmetic, local(): jnp.sum((picked * weights_flat[:, None]).reshape(group_rows, top_count, m...  9.96 us
  transfers between devices with their start and end apart: 6, of which 5 were waited for; matrix products, arithmetic and copies ran while one was open for 33% of the time, Pallas kernels for 0%

profile of v1, /device:TPU:0, one launch (start us, length us, event | category | flops | bytes accessed | tf_op | source)
XLA Modules:
  0.0 313.1 jit_solution(10703415528408597307)
XLA Ops:
  8.5 1.8 fusion.52
  13.1 2.4 scatter_custom_fusion
  15.6 14.3 %all-gather.3.cloned.1.call-done = bf16[256,2048]{1,0:T(8,128)(2,1)} async-done(((bf16[64,2048]{1,0:T(8,128)(2,1)}), bf16[256,2048]{1,0:T(8,128)(2,1)}) %all-gather.3.cloned.1.call-update) | async-done | bytes 1048592 | tf_op jit(solution)/shard_map/all_gather | solution.py:55
  29.9 1.3 concatenate.7
  31.2 6.0 %gather_fusion = bf16[1024,2048]{1,0:T(8,128)(2,1)} fusion(bf16[257,2048]{1,0:T(8,128)(2,1)S(1)} %concatenate.7, s32[1024]{0:T(1024)S(1)} %fusion.64), kind=kCustom, calls=%fused_computation | custom fusion | bytes 8392704 | tf_op jit(solution)/shard_map/gather | solution.py:68
  37.2 1.3 constant_dynamic-slice_fusion
  39.1 31.4 %all_to_all.10 = bf16[32,8,2048]{2,0,1:T(8,128)(2,1)S(1)} all-to-all(bf16[32,8,2048]{2,0,1:T(8,128)(2,1)S(1)} %copy.51), channel_id=1, replica_groups=mesh['ep'=8,'tp'=4] {'ep'}, dimensions={1} | all-to-all | bytes 2097152 | tf_op jit(solution)/shard_map/all_to_all | solution.py:71
  70.5 1.6 copy.40
  72.2 3.4 %collective-permute-start = (bf16[30,512]{1,0:T(8,128)(2,1)S(1)}, bf16[30,512]{1,0:T(8,128)(2,1)S(1)}, u32[]{:S(2)}, u32[]{:S(2)}) collective-permute-start(bf16[30,512]{1,0:T(8,128)(2,1)S(1)} %slice.192), channel_id=1, source_target_pairs={{0,4},{4,8},{8,12},{12,16},{16,20},{20,24},{24,28},{1,5},{5,9},{9,... | collective-permute-start | bytes 92168 | tf_op jit(solution)/shard_map/ppermute | solution.py:10
  75.6 1.5 collective-permute-done
  77.1 11.2 %fusion.72 = (f32[1024]{0:T(1024)S(1)}, f32[1024]{0:T(1024)S(1)}, f32[1024,512]{1,0:T(8,128)}) fusion(f32[512]{0:T(512)S(1)} %bitcast.138, bf16[1024,512]{1,0:T(8,128)(2,1)S(1)} %copy-done.2, f32[512]{0:T(512)S(1)} %bitcast.137, bf16[30,512]{1,0:T(8,128)(2,1)S(1)} %collective-permute-done, f32[512]{0:T(512)S(1)} %bitcast.136, f32[512]{0:T(512)S(1)} %bitcast.135, ...), kind=kLoop, calls=%fused_computation.135 | loop fusion | flops 96991232 | bytes 3248128 | tf_op jit(solution)/shard_map/reduce_sum | solution.py:38
  88.3 7.0 %all-reduce.1 = (f32[1024]{0:T(1024)S(1)}, f32[1024]{0:T(1024)S(1)}) all-reduce(f32[1024]{0:T(1024)S(1)} %get-tuple-element.3, f32[1024]{0:T(1024)S(1)} %get-tuple-element.2), channel_id=1, replica_groups=mesh['ep'=8,'tp'=4] {'tp'}, use_global_device_ids=true, to_apply=%region_3.0 | all-reduce | flops 2048 | bytes 16384 | tf_op jit(solution)/shard_map/psum | solution.py:38
  95.3 6.3 %convolution_convert_fusion = bf16[1024,2048]{1,0:T(8,128)(2,1)} fusion(bf16[512,2048]{1,0:T(8,128)(2,1)S(1)} %copy-done, f32[1024,512]{1,0:T(8,128)} %get-tuple-element.6, f32[512]{0:T(512)S(1)} %copy-done.6, f32[512]{0:T(512)S(1)} %copy-done.7, f32[1024]{0:T(1024)S(1)} %get-tuple-element.47, f32[1024]{0:T(1024)S(1)} %get-tuple-element.46), kind=kOutput, calls=%fused_computation.39 | convolution fusion | flops 2154299392 | bytes 8400896 | tf_op jit(solution)/shard_map/dot_general | solution.py:44
  101.6 3.5 %all-gather.5.cloned.1.call-done = bf16[128,8,2048]{2,1,0:T(8,128)(2,1)} async-done(((bf16[32,8,2048]{2,1,0:T(8,128)(2,1)}), bf16[128,8,2048]{2,1,0:T(8,128)(2,1)}) %all-gather.5.cloned.1.call-update) | async-done | bytes 4194320 | tf_op jit(solution)/shard_map/all_gather | solution.py:72
  105.1 5.9 %fusion.2 = f32[1024,512]{1,0:T(8,128)} fusion(bf16[128,8,2048]{2,1,0:T(8,128)(2,1)} %all-gather.5.cloned.1.call-done, bf16[1,2048,512]{2,1,0:T(8,128)(2,1)S(1)} %copy-done.5), kind=kOutput, calls=%fused_computation.34 | convolution fusion | flops 2147483648 | bytes 8388608 | tf_op jit(solution)/shard_map/dot_general | solution.py:74
  111.0 11.3 %convert_bitcast_fusion = bf16[128,8,2048]{2,1,0:T(8,128)(2,1)} fusion(bf16[1,512,2048]{2,1,0:T(8,128)(2,1)} %param.23, f32[1024,512]{1,0:T(8,128)} %fusion.2, bf16[1,2048,512]{2,1,0:T(8,128)(2,1)} %param.22, bf16[128,8,2048]{2,1,0:T(8,128)(2,1)} %all-gather.5.cloned.1.call-done), kind=kOutput, calls=%fused_computation.38 | convolution fusion | flops 4300210176 | bytes 14680064 | tf_op jit(solution)/shard_map/dot_general | solution.py:79
  122.3 22.6 %fusion.73 = (bf16[128,1,2048]{2,1,0:T(2,128)(2,1)S(1)}, bf16[128,1,2048]{2,1,0:T(2,128)(2,1)S(1)}, bf16[128,1,2048]{2,1,0:T(2,128)(2,1)S(1)}, bf16[128,1,2048]{...) fusion(bf16[128,8,2048]{2,1,0:T(8,128)(2,1)} %convert_bitcast_f, ...), kind=kLoop, calls=%fused_computation.136 | loop fusion | bytes 8388608 | tf_op jit(solution)/shard_map/split | solution.py:82
  153.9 5.7 %all-to-all-start.1 = ((bf16[8,128,1,2048]{3,1,2,0:T(8,128)(2,1)}), bf16[8,128,1,2048]{3,1,2,0:T(8,128)(2,1)}, u32[]{:S(2)}, u32[]{:S(2)}) async-start(bf16[8,128,1,2048]{3,1,2,0:T(8,128)(2,1)} %fusion.53), calls=%async_computation.2 | async-start | bytes 8388608 | tf_op jit(solution)/shard_map/all_to_all | solution.py:83
  159.8 93.5 %all-to-all-done.1 = bf16[8,128,1,2048]{3,1,2,0:T(8,128)(2,1)} async-done(((bf16[8,128,1,2048]{3,1,2,0:T(8,128)(2,1)}), bf16[8,128,1,2048]{3,1,2,0:T(8,128)(2,1)}, u32[]{:S(2)}, u32[]{:S(2)}) %all-to-all-start.1) | async-done | bytes 4194336 | tf_op jit(solution)/shard_map/all_to_all | solution.py:83
  253.2 6.5 %copy.85 = bf16[128,8,1,2048]{3,1,0,2:T(8,128)(2,1)} copy(bf16[128,8,1,2048]{3,0,2,1:T(8,128)(2,1)} %bitcast.49) | data formatting | bytes 8388608 | tf_op jit(solution)/shard_map/reshape | solution.py:84
  259.7 8.2 %gather_fusion.1 = bf16[512,2048]{1,0:T(8,128)(2,1)} fusion(bf16[1024,2048]{1,0:T(8,128)(2,1)} %bitcast.103, s32[1024]{0:T(1024)S(1)} %pad_clamp_fusion), kind=kCustom, calls=%fused_computation.1 | custom fusion | bytes 4196352 | tf_op jit(solution)/shard_map/gather | solution.py:85
  267.9 5.6 %reshape.95 = f32[256,2,2048]{2,1,0:T(2,128)} reshape(bf16[512,2048]{1,0:T(8,128)(2,1)} %gather_fusion.1) | data formatting | bytes 6291456 | tf_op jit(solution)/shard_map/convert_element_type | solution.py:85
  273.5 10.0 %multiply_reduce_fusion = bf16[256,2048]{1,0:T(8,128)(2,1)} fusion(f32[256,2,2048]{2,1,0:T(2,128)} %reshape.95, f32[256,2]{1,0:T(8,128)S(1)} %copy.50), kind=kLoop, calls=%fused_computation.37 | loop fusion | flops 1572864 | bytes 5244928 | tf_op jit(solution)/shard_map/reduce_sum | solution.py:86
  283.5 23.0 %reduce-scatter.5.cloned.1.call-done = bf16[64,2048]{1,0:T(8,128)(2,1)} async-done(((bf16[256,2048]{1,0:T(8,128)(2,1)}), bf16[64,2048]{1,0:T(8,128)(2,1)}) %reduce-scatter.5.cloned.1.call-update) | async-done | bytes 262160 | tf_op jit(solution)/shard_map/reduce_scatter | solution.py:89
  (56 shorter events, 14.0 us)
Async XLA Ops:
  7.2 88.1 %copy-start = (bf16[512,2048]{1,0:T(8,128)(2,1)S(1)}, bf16[512,2048]{1,0:T(8,128)(2,1)}, u32[]{:S(2)}) copy-start(bf16[512,2048]{1,0:T(8,128)(2,1)} %param.16) | copy-start | bytes 6291460
  7.2 22.7 %all-gather.3.cloned.1.call-start = ((), (), s32[]{:S(2)}) async-start(), calls=%async_computation.5 | async-start | bytes 1310720 | tf_op jit(solution)/shard_map/all_gather | solution.py:55
  10.3 94.8 %all-gather.5.cloned.1.call-start = ((), (), s32[]{:S(2)}) async-start(), calls=%async_computation.6 | async-start | bytes 5242880 | tf_op jit(solution)/shard_map/all_gather | solution.py:72
  70.5 1.6 copy-start.2
  70.5 5.0 %copy-start.3 = (bf16[31,512]{1,0:T(8,128)(2,1)S(1)}, bf16[31,512]{1,0:T(8,128)(2,1)}, u32[]{:S(2)}) copy-start(bf16[31,512]{1,0:T(8,128)(2,1)} %param.13) | copy-start | bytes 95236
  72.1 23.2 %copy-start.6 = (f32[512]{0:T(512)S(1)}, f32[512]{0:T(512)}, u32[]{:S(2)}) copy-start(f32[512]{0:T(512)} %param.15) | copy-start | bytes 6148
  72.1 23.2 %copy-start.7 = (f32[512]{0:T(512)S(1)}, f32[512]{0:T(512)}, u32[]{:S(2)}) copy-start(f32[512]{0:T(512)} %param.14) | copy-start | bytes 6148
  72.1 211.4 %reduce-scatter.3.cloned.1.call-start = ((), (), s32[]{:S(2)}) async-start(), calls=%async_computation.4 | async-start | bytes 5242880 | tf_op jit(solution)/shard_map/reduce_scatter | solution.py:43
  72.2 5.0 %collective-permute-start = (bf16[30,512]{1,0:T(8,128)(2,1)S(1)}, bf16[30,512]{1,0:T(8,128)(2,1)S(1)}, u32[]{:S(2)}, u32[]{:S(2)}) collective-permute-start(bf16[30,512]{1,0:T(8,128)(2,1)S(1)} %slice.192), channel_id=1, source_target_pairs={{0,4},{4,8},{8,12},{12,16},{16,20},{20,24},{24,28},{1,5},{5,9},{9,... | collective-permute-start | bytes 92168 | tf_op jit(solution)/shard_map/ppermute | solution.py:10
  101.6 3.5 %copy-start.5 = (bf16[1,2048,512]{2,1,0:T(8,128)(2,1)S(1)}, bf16[1,2048,512]{2,1,0:T(8,128)(2,1)}, u32[]{:S(2)}) copy-start(bf16[1,2048,512]{2,1,0:T(8,128)(2,1)} %param.21) | copy-start | bytes 6291460
  153.9 5.7 %copy-start.4 = (f32[256,2]{0,1:T(2,128)S(1)}, f32[256,2]{0,1:T(2,128)}, u32[]{:S(2)}) copy-start(f32[256,2]{0,1:T(2,128)} %param.20) | copy-start | bytes 6148
  153.9 99.3 %all-to-all-start.1 = ((bf16[8,128,1,2048]{3,1,2,0:T(8,128)(2,1)}), bf16[8,128,1,2048]{3,1,2,0:T(8,128)(2,1)}, u32[]{:S(2)}, u32[]{:S(2)}) async-start(bf16[8,128,1,2048]{3,1,2,0:T(8,128)(2,1)} %fusion.53), calls=%async_computation.2 | async-start | bytes 8388608 | tf_op jit(solution)/shard_map/all_to_all | solution.py:83
  159.5 147.0 %reduce-scatter.5.cloned.1.call-start = ((), (), s32[]{:S(2)}) async-start(), calls=%async_computation.7 | async-start | bytes 1310720 | tf_op jit(solution)/shard_map/reduce_scatter | solution.py:89
  267.9 38.6 %copy-start.1 = (bf16[512,2048]{1,0:T(8,128)(2,1)S(1)}, bf16[512,2048]{1,0:T(8,128)(2,1)}, u32[]{:S(2)}) copy-start(bf16[512,2048]{1,0:T(8,128)(2,1)} %param.16) | copy-start | bytes 6291460
Sparse Core Ops, SparseCore 0:
  10.4 19.4 all-gather.2
  72.2 32.8 all-gather.4
  108.2 44.5 reduce-scatter.2
  283.6 22.9 reduce-scatter.4
